TPU v7x, 32 devices: a whole 2x2x4 slice. The times are simulated.
32 devices in a mesh: kv: 8 (over z, y), tp: 4 (over x, core).
Axes of the slice: x: 2, y: 2, z: 4, core: 2. Of those that a mesh axis runs over, the one named last changes fastest.
Arguments:
- tokens: bfloat16 [4096, 2048], P('kv', 'tp'), may hold values from -9 to 9
- w_query: bfloat16 [2048, 1536], P(None, 'tp'), may hold values from -1 to 1
- w_key: bfloat16 [2048, 1536], P(None, 'tp'), may hold values from -1 to 1
- w_value: bfloat16 [2048, 1536], P(None, 'tp'), may hold values from -0.5 to 0.5
- w_out: bfloat16 [1536, 2048], P('tp'), may hold values from -0.15625 to 0.15625
- chosen: int32 [128, 24], P('kv'), may hold values from 0 to 127, as said below
Outputs:
- mixed: bfloat16 [4096, 2048], P(('kv', 'tp'))
Inputs may be any that keep to these rules, and one draw needn't show every extreme that they name: `chosen`: row c names blocks no later than c; its first entry is c and its second c - 1 (0 for row 0), and an entry may repeat. Taking the rows in aligned runs of 16, one run for each index of kv, the rows of one run name at most 2 distinct blocks lying in any one other index's positions; in every draw some index of kv names exactly 2 from every earlier index. Every run names some block of the index just before it and of the index half the axis before it, where those exist.
All inputs are finite; a program needn't handle non-finite values.
Results may differ from a plain program's by a relative error of at most 0.014.
Values may be sent and summed in bfloat16 or wider, within the bound.
A program may use at most 320 MiB of HBM per device.

v0:
```python
import jax
import jax.numpy as jnp
from jax import lax
from jax.sharding import PartitionSpec as P

HD = 128
BLK = 32
MOST = 2
NEG = -1e30


def attend(query_rows, key_rows, value_rows, block_ids, chosen, first_block):
    tok_rows, width = query_rows.shape
    head_count = width // HD
    key_count = key_rows.shape[0]
    slot_count = key_count // BLK
    query_blocks = tok_rows // BLK
    seen = (
        jnp.any(chosen[:, :, None] == block_ids[None, None, :], axis=1) & (block_ids >= 0)[None, :]
    )
    grid = jnp.broadcast_to(seen[:, None, :, None], (query_blocks, BLK, slot_count, BLK)).reshape(
        tok_rows, key_count
    )
    key_pos = (block_ids[:, None] * BLK + jnp.arange(BLK, dtype=jnp.int32)[None, :]).reshape(
        key_count
    )
    query_pos = first_block * BLK + jnp.arange(tok_rows, dtype=jnp.int32)
    allowed = grid & (key_pos[None, :] <= query_pos[:, None])
    query_heads = query_rows.reshape(tok_rows, head_count, HD)
    key_heads = key_rows.reshape(key_count, head_count, HD)
    value_heads = value_rows.reshape(key_count, head_count, HD)
    scores = jnp.einsum(
        "qhd,khd->hqk", query_heads, key_heads, preferred_element_type=jnp.float32
    ) * HD ** (-0.5)
    scores = jnp.where(allowed[None], scores, NEG)
    highest = jnp.max(scores, axis=-1)
    weights = jnp.where(allowed[None], jnp.exp(scores - highest[..., None]), 0.0)
    totals = jnp.sum(weights, axis=-1)
    summed = jnp.einsum("hqk,khd->hqd", weights, value_heads.astype(jnp.float32))
    return (highest, totals, summed)


def combine(left, right):
    highest = jnp.maximum(left[0], right[0])
    left_scale = jnp.exp(left[0] - highest)
    right_scale = jnp.exp(right[0] - highest)
    totals = left[1] * left_scale + right[1] * right_scale
    summed = left[2] * left_scale[..., None] + right[2] * right_scale[..., None]
    return (highest, totals, summed)


def local(tokens, w_query, w_key, w_value, w_out, chosen):
    tok_rows = tokens.shape[0]
    width = w_query.shape[1]
    empty = jnp.zeros((tok_rows, width), jnp.float32)
    totals = (empty, empty, empty)
    piece = lax.all_gather(tokens, "tp", axis=1, tiled=True)
    outputs = []
    for total, weight in zip(totals, (w_query, w_key, w_value)):
        rows = weight
        outputs.append(jnp.dot(piece, rows, preferred_element_type=jnp.float32))
    query_full, key_full, value_full = tuple(outputs)
    query_rows = query_full.astype(jnp.bfloat16)
    key_rows = key_full.astype(jnp.bfloat16)
    value_rows = value_full.astype(jnp.bfloat16)
    per_dev = tok_rows // BLK
    my_index = lax.axis_index("kv")
    first_block = my_index * per_dev
    own_ids = first_block + jnp.arange(per_dev, dtype=jnp.int32)
    own_part = attend(query_rows, key_rows, value_rows, own_ids, chosen, first_block)
    peers = lax.axis_size("kv")
    block_total = peers * per_dev
    wanted = jnp.any(
        chosen[:, :, None] == jnp.arange(block_total, dtype=jnp.int32)[None, None, :], axis=(0, 1)
    )
    peer_ids = jnp.arange(peers, dtype=jnp.int32)
    wanted = wanted.reshape(peers, per_dev) & (peer_ids != my_index)[:, None]
    ranks = jnp.cumsum(wanted.astype(jnp.int32), axis=1) - 1
    slot_hit = wanted[:, :, None] & (
        ranks[:, :, None] == jnp.arange(MOST, dtype=jnp.int32)[None, None, :]
    )
    local_ids = jnp.sum(
        slot_hit.astype(jnp.int32) * jnp.arange(per_dev, dtype=jnp.int32)[None, :, None], axis=1
    )
    present = jnp.any(slot_hit, axis=1)
    request = jnp.where(present, local_ids, -1)
    asked = lax.all_to_all(request, "kv", split_axis=0, concat_axis=0, tiled=True)
    picked = jnp.clip(asked, 0).reshape(-1)
    send_keys = key_rows.reshape(per_dev, BLK, width)[picked]
    send_values = value_rows.reshape(per_dev, BLK, width)[picked]
    got_keys, got_values = (
        lax.all_to_all(send_keys, "kv", split_axis=0, concat_axis=0, tiled=True),
        lax.all_to_all(send_values, "kv", split_axis=0, concat_axis=0, tiled=True),
    )
    got_ids = jnp.where(present, peer_ids[:, None] * per_dev + local_ids, -1).reshape(-1)
    far_part = attend(
        query_rows,
        got_keys.reshape(-1, width),
        got_values.reshape(-1, width),
        got_ids,
        chosen,
        first_block,
    )
    merged = combine(own_part, far_part)
    normed = merged[2] / merged[1][..., None]
    attended = jnp.transpose(normed, (1, 0, 2)).reshape(tok_rows, width).astype(jnp.bfloat16)
    rows = attended
    return lax.psum_scatter(
        jnp.dot(rows, w_out, preferred_element_type=jnp.float32).astype(jnp.bfloat16),
        "tp",
        scatter_dimension=0,
        tiled=True,
    )


def solution(mesh):
    return jax.shard_map(
        local,
        mesh=mesh,
        in_specs=(
            P("kv", "tp"),
            P(None, "tp"),
            P(None, "tp"),
            P(None, "tp"),
            P("tp", None),
            P("kv", None),
        ),
        out_specs=P(("kv", "tp"), None),
        check_vma=False,
    )
```

profile of v0, /device:TPU:0, one launch (start us, length us, event | category | flops | bytes accessed | tf_op | source)
XLA Modules:
  0.0 118.5 jit_solution(13071488536581529827)
XLA Ops:
  7.3 0.8 fusion.26
  9.4 7.3 %all-to-all-start = ((s32[8,1,2]{2,1,0:T(1,128)}), s32[8,1,2]{2,1,0:T(1,128)S(1)}, u32[]{:S(2)}, u32[]{:S(2)}) async-start(s32[8,1,2]{2,1,0:T(1,128)} %copy.46), calls=%async_computation | async-start | bytes 8192 | tf_op jit(solution)/shard_map/all_to_all | solution.py:87
  16.9 1.4 %compare_reduce_fusion = (pred[16,16]{1,0:T(8,128)(4,1)S(1)}, pred[16,16]{1,0:T(8,128)(4,1)S(1)}) fusion(s32[16,24]{1,0:T(8,128)} %param.11, s32[16]{0:T(128)S(1)} %select_n.53, s32[16]{0:T(128)S(1)} %get-tuple-element.20), kind=kLoop, calls=%fused_computation.40 | loop fusion | flops 24064 | bytes 2176 | tf_op jit(solution)/shard_map/reduce_or | solution.py:19
  18.8 2.1 %reshape.338 = pred[512,512]{0,1:T(8,128)(4,1)S(1)} reshape(pred[16,32,16,32]{1,0,3,2:T(8,128)(4,1)S(1)} %broadcast_in_dim.42) | data formatting | bytes 524288 | tf_op jit(solution)/shard_map/reshape | solution.py:21
  21.5 2.1 %reshape.333 = pred[512,512]{0,1:T(8,128)(4,1)S(1)} reshape(pred[16,32,16,32]{1,0,3,2:T(8,128)(4,1)S(1)} %broadcast_in_dim.37) | data formatting | bytes 524288 | tf_op jit(solution)/shard_map/reshape | solution.py:21
  24.4 9.8 %all-gather.2.cloned.1.call-done = bf16[512,2048]{1,0:T(8,128)(2,1)} async-done(((bf16[512,512]{1,0:T(8,128)(2,1)}), bf16[512,2048]{1,0:T(8,128)(2,1)}) %all-gather.2.cloned.1.call-update) | async-done | bytes 2097168 | tf_op jit(solution)/shard_map/all_gather | solution.py:57
  34.2 3.3 %convolution_convert_fusion.1 = bf16[512,384]{1,0:T(8,128)(2,1)S(1)} fusion(bf16[512,2048]{1,0:T(8,128)(2,1)} %all-gather.2.cloned.1.call-done, bf16[2048,384]{1,0:T(8,128)(2,1)} %param.9), kind=kOutput, calls=%fused_computation.28 | convolution fusion | flops 805502976 | bytes 4063232 | tf_op jit(solution)/shard_map/dot_general | solution.py:61
  37.5 0.9 copy.42
  38.4 3.3 %convolution_convert_fusion.2 = bf16[512,384]{1,0:T(8,128)(2,1)S(1)} fusion(bf16[512,2048]{1,0:T(8,128)(2,1)} %all-gather.2.cloned.1.call-done, bf16[2048,384]{1,0:T(8,128)(2,1)} %param.8), kind=kOutput, calls=%fused_computation.29 | convolution fusion | flops 805502976 | bytes 4063232 | tf_op jit(solution)/shard_map/dot_general | solution.py:61
  41.9 1.3 %gather_fusion = bf16[16,32,384]{2,1,0:T(8,128)(2,1)} fusion(bf16[16,32,384]{2,1,0:T(8,128)(2,1)S(1)} %bitcast.62, s32[1024]{0:T(1024)S(1)} %pad_clamp_fusion), kind=kCustom, calls=%fused_computation | custom fusion | bytes 786496 | tf_op jit(solution)/shard_map/gather | solution.py:89
  43.3 5.5 %all-to-all-start.1 = ((bf16[16,32,384]{2,1,0:T(8,128)(2,1)}), bf16[16,32,384]{2,1,0:T(8,128)(2,1)S(1)}, u32[]{:S(2)}, u32[]{:S(2)}) async-start(bf16[16,32,384]{2,1,0:T(8,128)(2,1)} %gather_fusion), calls=%async_computation.1 | async-start | bytes 786432 | tf_op jit(solution)/shard_map/all_to_all | solution.py:92
  48.8 1.4 %gather_fusion.1 = bf16[16,32,384]{2,1,0:T(8,128)(2,1)} fusion(bf16[16,32,384]{2,1,0:T(8,128)(2,1)S(1)} %bitcast.61, s32[1024]{0:T(1024)S(1)} %pad_clamp_fusion), kind=kCustom, calls=%fused_computation.1 | custom fusion | bytes 786496 | tf_op jit(solution)/shard_map/gather | solution.py:90
  50.2 3.1 %convolution_convert_fusion.3 = bf16[512,384]{0,1:T(8,128)(2,1)S(1)} fusion(bf16[512,2048]{1,0:T(8,128)(2,1)} %all-gather.2.cloned.1.call-done, bf16[2048,384]{1,0:T(8,128)(2,1)} %param.7), kind=kOutput, calls=%fused_computation.30 | convolution fusion | flops 805502976 | bytes 4063232 | tf_op jit(solution)/shard_map/dot_general | solution.py:61
  54.1 1.7 %copy-done.1 = f32[3,512,512]{1,2,0:T(8,128)} copy-done((f32[3,512,512]{1,2,0:T(8,128)}, f32[3,512,512]{1,2,0:T(8,128)S(1)}, u32[]{:S(2)}) %copy-start.1) | copy-done | bytes 3145752
  55.7 0.8 fusion.2
  56.5 4.3 %all-to-all-done.1 = bf16[16,32,384]{2,1,0:T(8,128)(2,1)S(1)} async-done(((bf16[16,32,384]{2,1,0:T(8,128)(2,1)}), bf16[16,32,384]{2,1,0:T(8,128)(2,1)S(1)}, u32[]{:S(2)}, u32[]{:S(2)}) %all-to-all-start.1) | async-done | bytes 393248 | tf_op jit(solution)/shard_map/all_to_all | solution.py:92
  60.9 3.6 %all-to-all-start.2 = ((bf16[16,32,384]{2,1,0:T(8,128)(2,1)}), bf16[16,32,384]{2,1,0:T(8,128)(2,1)S(1)}, u32[]{:S(2)}, u32[]{:S(2)}) async-start(bf16[16,32,384]{2,1,0:T(8,128)(2,1)} %gather_fusion.1), calls=%async_computation.2 | async-start | bytes 786432 | tf_op jit(solution)/shard_map/all_to_all | solution.py:93
  64.9 1.9 %fusion.1 = (f32[3,512]{1,0:T(4,128)S(1)}, f32[3,512,512]{1,2,0:T(8,128)S(1)}) fusion(pred[512,512]{0,1:T(8,128)(4,1)S(1)} %get-tuple-element.12, bf16[512,3,128]{0,2,1:T(8,128)(2,1)} %bitcast.64, bf16[512,3,128]{2,1,0:T(4,128)(2,1)S(1)} %reshape_reshape.6), kind=kOutput, calls=%fused_computation.8 | convolution fusion | flops 203684352 | bytes 4200448 | tf_op jit(solution)/shard_map/qhd,khd->hqk/dot_general | solution.py:32
  66.8 1.7 %copy-done.3 = f32[3,512,512]{1,2,0:T(8,128)} copy-done((f32[3,512,512]{1,2,0:T(8,128)}, f32[3,512,512]{1,2,0:T(8,128)S(1)}, u32[]{:S(2)}) %copy-start.3) | copy-done | bytes 3145752
  69.3 1.9 %fusion.18 = f32[512,3,128]{0,2,1:T(8,128)} fusion(bf16[512,3,128]{0,2,1:T(8,128)(2,1)S(1)} %bitcast.65, f32[3,512,512]{1,2,0:T(8,128)S(1)} %copy-done.2, f32[3,512]{1,0:T(4,128)S(1)} %get-tuple-element.16, pred[512,512]{0,1:T(8,128)(4,1)S(1)} %get-tuple-element.13, f32[512,3]{0,1:T(4,128)S(1)} %get-tuple-element.9), kind=kOutput, calls=%fused_computation.25 | convolution fusion | flops 204668928 | bytes 4599808 | tf_op jit(solution)/shard_map/hqk,khd->hqd/dot_general | solution.py:39
  71.2 5.2 %all-to-all-done.2 = bf16[16,32,384]{2,1,0:T(8,128)(2,1)S(1)} async-done(((bf16[16,32,384]{2,1,0:T(8,128)(2,1)}), bf16[16,32,384]{2,1,0:T(8,128)(2,1)S(1)}, u32[]{:S(2)}, u32[]{:S(2)}) %all-to-all-start.2) | async-done | bytes 393248 | tf_op jit(solution)/shard_map/all_to_all | solution.py:93
  76.5 3.1 %fusion.22 = bf16[512,3,128]{0,2,1:T(8,128)(2,1)S(1)} fusion(f32[512,3,128]{0,2,1:T(8,128)} %fusion.18, f32[3,512,512]{1,2,0:T(8,128)} %copy-done.3, f32[3,512]{1,0:T(4,128)S(1)} %get-tuple-element.18, pred[512,512]{0,1:T(8,128)(4,1)S(1)} %get-tuple-element.12, bf16[512,3,128]{2,1,0:T(4,128)(2,1)S(1)} %reshape_reshape.7, ...), kind=kOutput, calls=%fused_computation.34 | convolution fusion | flops 205258752 | bytes 4999168 | tf_op jit(solution)/shard_map/hqk,khd->hqd/dot_general | solution.py:39
  79.6 2.7 %convolution_convert_fusion = bf16[512,2048]{1,0:T(8,128)(2,1)} fusion(bf16[512,384]{0,1:T(8,128)(2,1)S(1)} %bitcast.66, bf16[384,2048]{1,0:T(8,128)(2,1)S(1)} %copy-done), kind=kOutput, calls=%fused_computation.6 | convolution fusion | flops 806354944 | bytes 4063232 | tf_op jit(solution)/shard_map/dot_general | solution.py:109
  82.3 29.4 %reduce-scatter.2.cloned.1.call-done = bf16[128,2048]{1,0:T(8,128)(2,1)} async-done(((bf16[512,2048]{1,0:T(8,128)(2,1)}), bf16[128,2048]{1,0:T(8,128)(2,1)}) %reduce-scatter.2.cloned.1.call-update) | async-done | bytes 524304 | tf_op jit(solution)/shard_map/reduce_scatter | solution.py:108
  (52 shorter events, 6.3 us)
Async XLA Ops:
  6.5 73.0 %copy-start = (bf16[384,2048]{1,0:T(8,128)(2,1)S(1)}, bf16[384,2048]{1,0:T(8,128)(2,1)}, u32[]{:S(2)}) copy-start(bf16[384,2048]{1,0:T(8,128)(2,1)} %param.10) | copy-start | bytes 4718596
  6.5 27.7 %all-gather.2.cloned.1.call-start = ((), (), s32[]{:S(2)}) async-start(), calls=%async_computation.4 | async-start | bytes 2621440 | tf_op jit(solution)/shard_map/all_gather | solution.py:57
  9.4 14.8 %all-to-all-start = ((s32[8,1,2]{2,1,0:T(1,128)}), s32[8,1,2]{2,1,0:T(1,128)S(1)}, u32[]{:S(2)}, u32[]{:S(2)}) async-start(s32[8,1,2]{2,1,0:T(1,128)} %copy.46), calls=%async_computation | async-start | bytes 8192 | tf_op jit(solution)/shard_map/all_to_all | solution.py:87
  43.3 17.6 %all-to-all-start.1 = ((bf16[16,32,384]{2,1,0:T(8,128)(2,1)}), bf16[16,32,384]{2,1,0:T(8,128)(2,1)S(1)}, u32[]{:S(2)}, u32[]{:S(2)}) async-start(bf16[16,32,384]{2,1,0:T(8,128)(2,1)} %gather_fusion), calls=%async_computation.1 | async-start | bytes 786432 | tf_op jit(solution)/shard_map/all_to_all | solution.py:92
  53.2 11.3 %copy-start.4 = (bf16[512,384]{0,1:T(8,128)(2,1)}, bf16[512,384]{0,1:T(8,128)(2,1)S(1)}, u32[]{:S(2)}) copy-start(bf16[512,384]{0,1:T(8,128)(2,1)S(1)} %convolution_convert_fusion.3) | copy-start | bytes 1179652
  54.0 1.7 %copy-start.1 = (f32[3,512,512]{1,2,0:T(8,128)}, f32[3,512,512]{1,2,0:T(8,128)S(1)}, u32[]{:S(2)}) copy-start(f32[3,512,512]{1,2,0:T(8,128)S(1)} %get-tuple-element.17) | copy-start | bytes 9437188
  60.9 15.5 %all-to-all-start.2 = ((bf16[16,32,384]{2,1,0:T(8,128)(2,1)}), bf16[16,32,384]{2,1,0:T(8,128)(2,1)S(1)}, u32[]{:S(2)}, u32[]{:S(2)}) async-start(bf16[16,32,384]{2,1,0:T(8,128)(2,1)} %gather_fusion.1), calls=%async_computation.2 | async-start | bytes 786432 | tf_op jit(solution)/shard_map/all_to_all | solution.py:93
  64.5 47.2 %reduce-scatter.2.cloned.1.call-start = ((), (), s32[]{:S(2)}) async-start(), calls=%async_computation.5 | async-start | bytes 2621440 | tf_op jit(solution)/shard_map/reduce_scatter | solution.py:108
  64.8 4.5 %copy-start.2 = (f32[3,512,512]{1,2,0:T(8,128)S(1)}, f32[3,512,512]{1,2,0:T(8,128)}, u32[]{:S(2)}) copy-start(f32[3,512,512]{1,2,0:T(8,128)} %copy-done.1) | copy-start | bytes 9437188
  64.9 4.5 %copy-start.5 = (bf16[512,384]{0,1:T(8,128)(2,1)S(1)}, bf16[512,384]{0,1:T(8,128)(2,1)}, u32[]{:S(2)}) copy-start(bf16[512,384]{0,1:T(8,128)(2,1)} %copy.42) | copy-start | bytes 1179652
  66.8 1.7 %copy-start.3 = (f32[3,512,512]{1,2,0:T(8,128)}, f32[3,512,512]{1,2,0:T(8,128)S(1)}, u32[]{:S(2)}) copy-start(f32[3,512,512]{1,2,0:T(8,128)S(1)} %get-tuple-element.19) | copy-start | bytes 9437188
Sparse Core Ops, SparseCore 0:
  8.9 25.2 all-gather.1
  82.4 29.2 reduce-scatter.1
where the time goes:
time: 119 us
  waiting for transfers between devices  49.5 us (42%)
  matrix products  19.9 us (17%)
  starting transfers between devices  16.7 us (14%)
  local copies, waits for them, and re-layouts  13.7 us (12%)
  between operations  13.6 us (11%)
  other arithmetic  5.12 us (4%)
    reduce_scatter x1, waiting for transfers between devices, local(): lax.psum_scatter(jnp.dot(rows, w_out, preferred_element_type=jnp.float32)...  29.4 us
    all_gather x1, waiting for transfers between devices, local(): piece = lax.all_gather(tokens, 'tp', axis=1, tiled=True)  9.83 us
    dot_general x3, matrix products, local(): outputs.append(jnp.dot(piece, rows, preferred_element_type=jnp.float32))  9.62 us
    all_to_all x1, starting transfers between devices, local(): lax.all_to_all(request, 'kv', split_axis=0, concat_axis=0, tiled=True)  7.31 us
    all_to_all x1, starting transfers between devices, local(): lax.all_to_all(send_keys, 'kv', split_axis=0, concat_axis=0, tiled=True)  5.51 us
    all_to_all x1, waiting for transfers between devices, local(): lax.all_to_all(send_values, 'kv', split_axis=0, concat_axis=0, tiled=True)  5.16 us
    dot_general x2, matrix products, attend(): jnp.einsum('hqk,khd->hqd', weights, value_heads.astype(jnp.float32))  4.96 us
    all_to_all x1, waiting for transfers between devices, local(): lax.all_to_all(send_keys, 'kv', split_axis=0, concat_axis=0, tiled=True)  4.32 us
  transfers between devices with their start and end apart: 5, of which 4 were waited for; matrix products, arithmetic and copies ran while one was open for 17% of the time, Pallas kernels for 0%

commit v1 on v0

--- a/solution.py
+++ b/solution.py
@@ -54,7 +54,12 @@
     width = w_query.shape[1]
     empty = jnp.zeros((tok_rows, width), jnp.float32)
     totals = (empty, empty, empty)
-    piece = lax.all_gather(tokens, "tp", axis=1, tiled=True)
+    ring = [tokens]
+    for hop in range(3):
+        ring.append(lax.ppermute(ring[-1], "tp", [(dev, (dev + 1) % 4) for dev in range(4)]))
+    piece = jnp.roll(
+        jnp.concatenate(ring[::-1], axis=1), (lax.axis_index("tp") + 1) * ring[0].shape[1], axis=1
+    )
     outputs = []
     for total, weight in zip(totals, (w_query, w_key, w_value)):
         rows = weight

time: 119 us -> 135 us (1.13)
  local copies, waits for them, and re-layouts: 13.7 us -> 25.6 us
  starting transfers between devices: 16.7 us -> 18.6 us
  other arithmetic: 5.12 us -> 6.76 us
    unnamed x12 -> x31, local copies, waits for them, and re-layouts: 3.37 us -> 13.8 us
    all_gather x1 -> x0, waiting for transfers between devices: 9.83 us -> none  [local(): piece = lax.all_gather(tokens, 'tp', axis=1, tiled=True)]
    ppermute x0 -> x3, waiting for transfers between devices: none -> 8.13 us  [local(): lax.ppermute(ring[-1], 'tp', [(dev, (dev + 1) % 4) for dev in range(4)])]
    all_to_all x1, waiting for transfers between devices: 4.32 us -> 8.01 us  [local(): lax.all_to_all(send_keys, 'kv', split_axis=0, concat_axis=0, tiled=True)]
    ppermute x0 -> x3, starting transfers between devices: none -> 1.75 us  [local(): lax.ppermute(ring[-1], 'tp', [(dev, (dev + 1) % 4) for dev in range(4)])]
    and x1, other arithmetic: 0.47 us -> 2.12 us  [attend(): allowed = grid & (key_pos[None, :] <= query_pos[:, None])]
  transfers between devices with their start and end apart: 5 -> 7, of which waited for: 4 -> 5; matrix products, arithmetic and copies ran while one was open for 17% -> 15% of each run, Pallas kernels for 0% -> 0%
where the time goes in v1:
time: 135 us
  waiting for transfers between devices  50.8 us (38%)
  local copies, waits for them, and re-layouts  25.6 us (19%)
  matrix products  19.3 us (14%)
  starting transfers between devices  18.6 us (14%)
  between operations  13.7 us (10%)
  other arithmetic  6.76 us (5%)
    reduce_scatter x1, waiting for transfers between devices, local(): lax.psum_scatter(jnp.dot(rows, w_out, preferred_element_type=jnp.float32)...  29.4 us
    unnamed x31, local copies, waits for them, and re-layouts  13.8 us
    dot_general x3, matrix products, local(): outputs.append(jnp.dot(piece, rows, preferred_element_type=jnp.float32))  9.02 us
    ppermute x3, waiting for transfers between devices, local(): lax.ppermute(ring[-1], 'tp', [(dev, (dev + 1) % 4) for dev in range(4)])  8.13 us
    all_to_all x1, waiting for transfers between devices, local(): lax.all_to_all(send_keys, 'kv', split_axis=0, concat_axis=0, tiled=True)  8.01 us
    all_to_all x1, starting transfers between devices, local(): lax.all_to_all(request, 'kv', split_axis=0, concat_axis=0, tiled=True)  6.94 us
    all_to_all x1, starting transfers between devices, local(): lax.all_to_all(send_keys, 'kv', split_axis=0, concat_axis=0, tiled=True)  6 us
    all_to_all x1, waiting for transfers between devices, local(): lax.all_to_all(send_values, 'kv', split_axis=0, concat_axis=0, tiled=True)  5.21 us
  transfers between devices with their start and end apart: 7, of which 5 were waited for; matrix products, arithmetic and copies ran while one was open for 15% of the time, Pallas kernels for 0%

profile of v1, /device:TPU:0, one launch (start us, length us, event | category | flops | bytes accessed | tf_op | source)
XLA Modules:
  0.0 134.7 jit_solution(17960989357913701587)
XLA Ops:
  9.2 6.9 %all-to-all-start = ((s32[8,1,2]{2,1,0:T(1,128)}), s32[8,1,2]{2,1,0:T(1,128)S(1)}, u32[]{:S(2)}, u32[]{:S(2)}) async-start(s32[8,1,2]{2,1,0:T(1,128)} %copy.46), calls=%async_computation | async-start | bytes 8192 | tf_op jit(solution)/shard_map/all_to_all | solution.py:92
  16.3 1.4 %compare_reduce_fusion = (pred[16,16]{1,0:T(8,128)(4,1)S(1)}, pred[16,16]{1,0:T(8,128)(4,1)S(1)}) fusion(s32[16,24]{1,0:T(8,128)} %param.11, s32[16]{0:T(128)S(1)} %select_n.68, s32[16]{0:T(128)S(1)} %get-tuple-element.20), kind=kLoop, calls=%fused_computation.46 | loop fusion | flops 24064 | bytes 2176 | tf_op jit(solution)/shard_map/reduce_or | solution.py:19
  19.2 7.4 %collective-permute-done.1 = bf16[512,512]{1,0:T(8,128)(2,1)} collective-permute-done((bf16[512,512]{1,0:T(8,128)(2,1)S(1)}, bf16[512,512]{1,0:T(8,128)(2,1)}, u32[]{:S(2)}, u32[]{:S(2)}) %collective-permute-start.1) | collective-permute-done | bytes 524320 | tf_op jit(solution)/shard_map/ppermute | solution.py:59
  27.0 2.1 %reshape.338 = pred[512,512]{0,1:T(8,128)(4,1)S(1)} reshape(pred[16,32,16,32]{1,0,3,2:T(8,128)(4,1)S(1)} %broadcast_in_dim.42) | data formatting | bytes 524288 | tf_op jit(solution)/shard_map/reshape | solution.py:21
  29.6 2.8 %reshape.333 = pred[512,512]{0,1:T(8,128)(4,1)} reshape(pred[16,32,16,32]{1,0,3,2:T(8,128)(4,1)S(1)} %broadcast_in_dim.37) | data formatting | bytes 524288 | tf_op jit(solution)/shard_map/reshape | solution.py:21
  32.5 2.1 %compare_and_fusion = (pred[512,512]{0,1:T(8,128)(4,1)}, pred[512,512]{0,1:T(8,128)(4,1)S(1)}) fusion(pred[512,512]{0,1:T(8,128)(4,1)S(1)} %reshape.338, s32[512]{0:T(512)S(1)} %iota_add_fusion.2, s32[512]{0:T(512)S(1)} %add.144, pred[512,512]{0,1:T(8,128)(4,1)} %reshape.333, s32[512]{0:T(512)S(1)} %add.133), kind=kLoop, calls=%fused_computation.37 | loop fusion | flops 1048576 | bytes 1054720 | tf_op jit(solution)/shard_map/and | solution.py:28
  35.5 1.9 %constant_dynamic-update-slice_fusion.7 = bf16[512,4096]{1,0:T(8,128)(2,1)} fusion(bf16[512,512]{1,0:T(8,128)(2,1)} %collective-permute-done.2), kind=kLoop, calls=%fused_computation.55 | loop fusion | bytes 1048576
  37.4 1.9 %constant_dynamic-update-slice_fusion.6 = bf16[512,4096]{1,0:T(8,128)(2,1)} fusion(bf16[512,4096]{1,0:T(8,128)(2,1)} %constant_dynamic-update-slice_fusion.7, bf16[512,512]{1,0:T(8,128)(2,1)} %collective-permute-done.1), kind=kLoop, calls=%fused_computation.54 | loop fusion | bytes 1048576
  41.1 2.0 %constant_dynamic-update-slice_fusion.3 = bf16[512,4096]{1,0:T(8,128)(2,1)} fusion(bf16[512,4096]{1,0:T(8,128)(2,1)} %constant_dynamic-update-slice_fusion.4, bf16[512,512]{1,0:T(8,128)(2,1)} %collective-permute-done.2), kind=kLoop, calls=%fused_computation.51 | loop fusion | bytes 1048576
  43.1 1.9 %constant_dynamic-update-slice_fusion.2 = bf16[512,4096]{1,0:T(8,128)(2,1)} fusion(bf16[512,4096]{1,0:T(8,128)(2,1)} %constant_dynamic-update-slice_fusion.3, bf16[512,512]{1,0:T(8,128)(2,1)} %collective-permute-done.1), kind=kLoop, calls=%fused_computation.50 | loop fusion | bytes 1048576
  46.7 2.8 %fusion.33 = bf16[512,384]{1,0:T(8,128)(2,1)S(1)} fusion(bf16[2048,384]{1,0:T(8,128)(2,1)S(1)} %copy-done.10, bf16[512,4096]{1,0:T(8,128)(2,1)} %constant_dynamic-update-slice_fusion, s32[]{:T(128)S(6)} %select_n.64), kind=kOutput, calls=%fused_computation.36 | convolution fusion | flops 805502976 | bytes 4063236 | tf_op jit(solution)/shard_map/dot_general | solution.py:66
  50.5 3.2 %fusion.27 = bf16[512,384]{0,1:T(8,128)(2,1)S(1)} fusion(bf16[2048,384]{1,0:T(8,128)(2,1)} %param.7, bf16[512,4096]{1,0:T(8,128)(2,1)} %constant_dynamic-update-slice_fusion, s32[]{:T(128)S(6)} %select_n.64), kind=kOutput, calls=%fused_computation.34 | convolution fusion | flops 805502976 | bytes 4063236 | tf_op jit(solution)/shard_map/dot_general | solution.py:66
  53.7 3.0 %fusion.30 = bf16[512,384]{1,0:T(8,128)(2,1)S(1)} fusion(bf16[2048,384]{1,0:T(8,128)(2,1)S(1)} %copy-done.11, bf16[512,4096]{1,0:T(8,128)(2,1)} %constant_dynamic-update-slice_fusion, s32[]{:T(128)S(6)} %select_n.64), kind=kOutput, calls=%fused_computation.35 | convolution fusion | flops 805502976 | bytes 4063236 | tf_op jit(solution)/shard_map/dot_general | solution.py:66
  58.3 6.0 %all-to-all-start.1 = ((bf16[16,32,384]{2,1,0:T(8,128)(2,1)}), bf16[16,32,384]{2,1,0:T(8,128)(2,1)S(1)}, u32[]{:S(2)}, u32[]{:S(2)}) async-start(bf16[16,32,384]{2,1,0:T(8,128)(2,1)} %gather_fusion), calls=%async_computation.1 | async-start | bytes 786432 | tf_op jit(solution)/shard_map/all_to_all | solution.py:97
  66.5 1.6 %copy-done.1 = f32[3,512,512]{1,2,0:T(8,128)} copy-done((f32[3,512,512]{1,2,0:T(8,128)}, f32[3,512,512]{1,2,0:T(8,128)S(1)}, u32[]{:S(2)}) %copy-start.1) | copy-done | bytes 3145752
  69.0 8.0 %all-to-all-done.1 = bf16[16,32,384]{2,1,0:T(8,128)(2,1)S(1)} async-done(((bf16[16,32,384]{2,1,0:T(8,128)(2,1)}), bf16[16,32,384]{2,1,0:T(8,128)(2,1)S(1)}, u32[]{:S(2)}, u32[]{:S(2)}) %all-to-all-start.1) | async-done | bytes 393248 | tf_op jit(solution)/shard_map/all_to_all | solution.py:97
  77.0 3.6 %all-to-all-start.2 = ((bf16[16,32,384]{2,1,0:T(8,128)(2,1)}), bf16[16,32,384]{2,1,0:T(8,128)(2,1)S(1)}, u32[]{:S(2)}, u32[]{:S(2)}) async-start(bf16[16,32,384]{2,1,0:T(8,128)(2,1)} %gather_fusion.1), calls=%async_computation.2 | async-start | bytes 786432 | tf_op jit(solution)/shard_map/all_to_all | solution.py:98
  81.0 1.9 %fusion.1 = (f32[3,512]{1,0:T(4,128)S(1)}, f32[3,512,512]{1,2,0:T(8,128)S(1)}) fusion(pred[512,512]{0,1:T(8,128)(4,1)S(1)} %copy-done.7, bf16[512,3,128]{0,2,1:T(8,128)(2,1)} %bitcast.61, bf16[512,3,128]{2,1,0:T(4,128)(2,1)S(1)} %reshape_reshape.6), kind=kOutput, calls=%fused_computation.8 | convolution fusion | flops 203684352 | bytes 4200448 | tf_op jit(solution)/shard_map/qhd,khd->hqk/dot_general | solution.py:32
  82.9 1.7 %copy-done.3 = f32[3,512,512]{1,2,0:T(8,128)} copy-done((f32[3,512,512]{1,2,0:T(8,128)}, f32[3,512,512]{1,2,0:T(8,128)S(1)}, u32[]{:S(2)}) %copy-start.3) | copy-done | bytes 3145752
  85.5 1.9 %fusion.24 = f32[512,3,128]{0,2,1:T(8,128)} fusion(bf16[512,3,128]{0,2,1:T(8,128)(2,1)S(1)} %bitcast.62, f32[3,512,512]{1,2,0:T(8,128)S(1)} %copy-done.2, f32[3,512]{1,0:T(4,128)S(1)} %get-tuple-element.16, pred[512,512]{0,1:T(8,128)(4,1)S(1)} %get-tuple-element.13, f32[512,3]{0,1:T(4,128)S(1)} %get-tuple-element.9), kind=kOutput, calls=%fused_computation.31 | convolution fusion | flops 204668928 | bytes 4599808 | tf_op jit(solution)/shard_map/hqk,khd->hqd/dot_general | solution.py:39
  87.3 5.2 %all-to-all-done.2 = bf16[16,32,384]{2,1,0:T(8,128)(2,1)S(1)} async-done(((bf16[16,32,384]{2,1,0:T(8,128)(2,1)}), bf16[16,32,384]{2,1,0:T(8,128)(2,1)S(1)}, u32[]{:S(2)}, u32[]{:S(2)}) %all-to-all-start.2) | async-done | bytes 393248 | tf_op jit(solution)/shard_map/all_to_all | solution.py:98
  92.6 3.1 %fusion.37 = bf16[512,3,128]{0,2,1:T(8,128)(2,1)S(1)} fusion(f32[512,3,128]{0,2,1:T(8,128)} %fusion.24, f32[3,512,512]{1,2,0:T(8,128)} %copy-done.3, f32[3,512]{1,0:T(4,128)S(1)} %get-tuple-element.18, pred[512,512]{0,1:T(8,128)(4,1)S(1)} %copy-done.7, bf16[512,3,128]{2,1,0:T(4,128)(2,1)S(1)} %reshape_reshape.7, f32[512,3]{0,1:T(4,128)S(1)} %get-tuple-element.7, ...), kind=kOutput, calls=%fused_computation.40 | convolution fusion | flops 205258752 | bytes 4999168 | tf_op jit(solution)/shard_map/hqk,khd->hqd/dot_general | solution.py:39
  95.7 2.7 %convolution_convert_fusion = bf16[512,2048]{1,0:T(8,128)(2,1)} fusion(bf16[512,384]{0,1:T(8,128)(2,1)S(1)} %bitcast.63, bf16[384,2048]{1,0:T(8,128)(2,1)S(1)} %copy-done), kind=kOutput, calls=%fused_computation.6 | convolution fusion | flops 806354944 | bytes 4063232 | tf_op jit(solution)/shard_map/dot_general | solution.py:114
  98.4 29.4 %reduce-scatter.2.cloned.1.call-done = bf16[128,2048]{1,0:T(8,128)(2,1)} async-done(((bf16[512,2048]{1,0:T(8,128)(2,1)}), bf16[128,2048]{1,0:T(8,128)(2,1)}) %reduce-scatter.2.cloned.1.call-update) | async-done | bytes 524304 | tf_op jit(solution)/shard_map/reduce_scatter | solution.py:113
  (75 shorter events, 16.5 us)
Async XLA Ops:
  6.5 89.2 %copy-start = (bf16[384,2048]{1,0:T(8,128)(2,1)S(1)}, bf16[384,2048]{1,0:T(8,128)(2,1)}, u32[]{:S(2)}) copy-start(bf16[384,2048]{1,0:T(8,128)(2,1)} %param.10) | copy-start | bytes 4718596
  6.5 11.2 %collective-permute-start = (bf16[512,512]{1,0:T(8,128)(2,1)}, bf16[512,512]{1,0:T(8,128)(2,1)S(1)}, u32[]{:S(2)}, u32[]{:S(2)}) collective-permute-start(bf16[512,512]{1,0:T(8,128)(2,1)} %param.6), channel_id=1, source_target_pairs={{0,1},{1,2},{2,3},{3,0},{4,5},{5,6},{6,7},{7,4},{8,9},{9,10},{10,1... | collective-permute-start | bytes 1572872 | tf_op jit(solution)/shard_map/ppermute | solution.py:59
  9.2 25.4 %all-to-all-start = ((s32[8,1,2]{2,1,0:T(1,128)}), s32[8,1,2]{2,1,0:T(1,128)S(1)}, u32[]{:S(2)}, u32[]{:S(2)}) async-start(s32[8,1,2]{2,1,0:T(1,128)} %copy.46), calls=%async_computation | async-start | bytes 8192 | tf_op jit(solution)/shard_map/all_to_all | solution.py:92
  17.8 8.8 %copy-start.5 = (bf16[512,512]{1,0:T(8,128)(2,1)}, bf16[512,512]{1,0:T(8,128)(2,1)S(1)}, u32[]{:S(2)}) copy-start(bf16[512,512]{1,0:T(8,128)(2,1)S(1)} %collective-permute-done) | copy-start | bytes 1572868
  17.8 8.8 %collective-permute-start.1 = (bf16[512,512]{1,0:T(8,128)(2,1)S(1)}, bf16[512,512]{1,0:T(8,128)(2,1)}, u32[]{:S(2)}, u32[]{:S(2)}) collective-permute-start(bf16[512,512]{1,0:T(8,128)(2,1)S(1)} %collective-permute-done), channel_id=1, source_target_pairs={{0,1},{1,2},{2,3},{3,0},{4,5},{5,6},{6,7},{7,4},{8,9},{9,10},{10,1... | collective-permute-start | bytes 1572872 | tf_op jit(solution)/shard_map/ppermute | solution.py:59
  26.6 8.9 %collective-permute-start.2 = (bf16[512,512]{1,0:T(8,128)(2,1)}, bf16[512,512]{1,0:T(8,128)(2,1)}, u32[]{:S(2)}, u32[]{:S(2)}) collective-permute-start(bf16[512,512]{1,0:T(8,128)(2,1)} %collective-permute-done.1), channel_id=1, source_target_pairs={{0,1},{1,2},{2,3},{3,0},{4,5},{5,6},{6,7},{7,4},{8,9},{9,10},{10,1... | collective-permute-start | bytes 1572872 | tf_op jit(solution)/shard_map/ppermute | solution.py:59
  29.3 10.9 %copy-start.4 = (bf16[512,512]{1,0:T(8,128)(2,1)S(1)}, bf16[512,512]{1,0:T(8,128)(2,1)}, u32[]{:S(2)}) copy-start(bf16[512,512]{1,0:T(8,128)(2,1)} %param.6) | copy-start | bytes 1572868
  32.4 6.9 %copy-start.6 = (bf16[512,512]{1,0:T(8,128)(2,1)S(1)}, bf16[512,512]{1,0:T(8,128)(2,1)}, u32[]{:S(2)}) copy-start(bf16[512,512]{1,0:T(8,128)(2,1)} %copy-done.5) | copy-start | bytes 1572868
  39.3 7.4 %copy-start.10 = (bf16[2048,384]{1,0:T(8,128)(2,1)S(1)}, bf16[2048,384]{1,0:T(8,128)(2,1)}, u32[]{:S(2)}) copy-start(bf16[2048,384]{1,0:T(8,128)(2,1)} %param.9) | copy-start | bytes 4718596
  50.5 3.2 %copy-start.11 = (bf16[2048,384]{1,0:T(8,128)(2,1)S(1)}, bf16[2048,384]{1,0:T(8,128)(2,1)}, u32[]{:S(2)}) copy-start(bf16[2048,384]{1,0:T(8,128)(2,1)} %param.8) | copy-start | bytes 4718596
  53.7 26.9 %copy-start.8 = (bf16[512,384]{0,1:T(8,128)(2,1)}, bf16[512,384]{0,1:T(8,128)(2,1)S(1)}, u32[]{:S(2)}) copy-start(bf16[512,384]{0,1:T(8,128)(2,1)S(1)} %fusion.27) | copy-start | bytes 1179652
  58.3 18.7 %all-to-all-start.1 = ((bf16[16,32,384]{2,1,0:T(8,128)(2,1)}), bf16[16,32,384]{2,1,0:T(8,128)(2,1)S(1)}, u32[]{:S(2)}, u32[]{:S(2)}) async-start(bf16[16,32,384]{2,1,0:T(8,128)(2,1)} %gather_fusion), calls=%async_computation.1 | async-start | bytes 786432 | tf_op jit(solution)/shard_map/all_to_all | solution.py:97
  66.5 1.7 %copy-start.1 = (f32[3,512,512]{1,2,0:T(8,128)}, f32[3,512,512]{1,2,0:T(8,128)S(1)}, u32[]{:S(2)}) copy-start(f32[3,512,512]{1,2,0:T(8,128)S(1)} %get-tuple-element.17) | copy-start | bytes 9437188
  66.5 14.5 %copy-start.7 = (pred[512,512]{0,1:T(8,128)(4,1)S(1)}, pred[512,512]{0,1:T(8,128)(4,1)}, u32[]{:S(2)}) copy-start(pred[512,512]{0,1:T(8,128)(4,1)} %get-tuple-element.12) | copy-start | bytes 786436
  77.0 15.6 %all-to-all-start.2 = ((bf16[16,32,384]{2,1,0:T(8,128)(2,1)}), bf16[16,32,384]{2,1,0:T(8,128)(2,1)S(1)}, u32[]{:S(2)}, u32[]{:S(2)}) async-start(bf16[16,32,384]{2,1,0:T(8,128)(2,1)} %gather_fusion.1), calls=%async_computation.2 | async-start | bytes 786432 | tf_op jit(solution)/shard_map/all_to_all | solution.py:98
  80.6 47.2 %reduce-scatter.2.cloned.1.call-start = ((), (), s32[]{:S(2)}) async-start(), calls=%async_computation.4 | async-start | bytes 2621440 | tf_op jit(solution)/shard_map/reduce_scatter | solution.py:113
  81.0 4.5 %copy-start.2 = (f32[3,512,512]{1,2,0:T(8,128)S(1)}, f32[3,512,512]{1,2,0:T(8,128)}, u32[]{:S(2)}) copy-start(f32[3,512,512]{1,2,0:T(8,128)} %copy-done.1) | copy-start | bytes 9437188
  81.0 4.5 %copy-start.9 = (bf16[512,384]{0,1:T(8,128)(2,1)S(1)}, bf16[512,384]{0,1:T(8,128)(2,1)}, u32[]{:S(2)}) copy-start(bf16[512,384]{0,1:T(8,128)(2,1)} %copy.42) | copy-start | bytes 1179652
  82.9 1.7 %copy-start.3 = (f32[3,512,512]{1,2,0:T(8,128)}, f32[3,512,512]{1,2,0:T(8,128)S(1)}, u32[]{:S(2)}) copy-start(f32[3,512,512]{1,2,0:T(8,128)S(1)} %get-tuple-element.19) | copy-start | bytes 9437188
Sparse Core Ops, SparseCore 0:
  98.5 29.2 reduce-scatter.1
